TPU v7x, 32 devices: a whole 2x2x4 slice. The times are simulated.
32 devices in a mesh: sp: 8 (over z, x), dp: 4 (over y, core).
Axes of the slice: x: 2, y: 2, z: 4, core: 2. Of those that a mesh axis runs over, the one named last changes fastest.
Arguments:
- queries: bfloat16 [4, 1024, 2048], P('dp', 'sp'), may hold values from -12 to 12
- key_rows: bfloat16 [4, 1024, 2048], P('dp', 'sp'), may hold values from -12 to 12
- value_rows: bfloat16 [4, 1024, 2048], P('dp', 'sp'), may hold values from -6 to 6
- lambdas: float32 [16], P('sp'), may hold values from 0.3 to 0.8
- head_gain: float32 [128], replicated, may hold values from 0.1 to 1.9
- out_weight: bfloat16 [2048, 2048], replicated, may hold values from -0.125 to 0.125
- residual: bfloat16 [4, 1024, 2048], P('dp', 'sp'), may hold values from -6 to 6
- mixer_gain: float32 [2048], replicated, may hold values from 0.1 to 1.9
- channel_gain: float32 [2048], replicated, may hold values from 0.1 to 1.9
- expert_gain: float32 [2048], replicated, may hold values from 0.1 to 1.9
- routes: int32 [4, 1024, 2], P('dp', 'sp'), may hold values from 0 to 7, all different within a row; in each aligned block of 128 rows (0 to 127, 128 to 255, ..., all dimensions but the last counted through in order) at most 48 rows name the same one
- route_logits: float32 [4, 1024, 2], P('dp', 'sp'), may hold values from -5 to 5
- gate_weight: bfloat16 [8, 2048, 4096], P('sp', None, 'dp'), may hold values from -0.125 to 0.125
- up_weight: bfloat16 [8, 2048, 4096], P('sp', None, 'dp'), may hold values from -0.125 to 0.125
- down_weight: bfloat16 [8, 4096, 2048], P('sp', 'dp'), may hold values from -0.09375 to 0.09375
Outputs:
- updated: bfloat16 [4, 1024, 2048], P('dp', 'sp')
Inputs may be any that keep to these rules, and one draw needn't show every extreme that they name: `routes`: among the rows of one device no expert is named by more than 48 rows; in some of these blocks one expert is named by exactly 48.
All inputs are finite; a program needn't handle non-finite values.
Results may differ from a plain program's by a relative error of at most 0.014.
Values may be sent and summed in bfloat16 or wider, within the bound.
A program may use at most 128 MiB of HBM per device.

v0:
```python
import math
import jax
import jax.numpy as jnp
from jax import lax
from jax.sharding import PartitionSpec as P


def rotate(field):
    dim_full = field.shape[-1]
    dim_half = dim_full // 2
    inverse = 1.0 / 10000.0 ** (jnp.arange(0, dim_full, 2, dtype=jnp.float32) / dim_full)
    angles = jnp.arange(field.shape[-4], dtype=jnp.float32)[:, None] * inverse[None, :]
    cosine = jnp.cos(angles)[:, None, None, :]
    sine_table = jnp.sin(angles)[:, None, None, :]
    floats = field.astype(jnp.float32)
    front_part = floats[..., :dim_half]
    second = floats[..., dim_half:]
    turned = jnp.concatenate(
        [front_part * cosine - second * sine_table, second * cosine + front_part * sine_table],
        axis=-1,
    )
    return turned.astype(jnp.bfloat16)


def rms_scale(values, epsilon):
    return values * lax.rsqrt(jnp.mean(values * values, axis=-1, keepdims=True) + epsilon)


def local(
    queries,
    key_rows,
    value_rows,
    lambdas,
    head_gain,
    out_weight,
    residual,
    mixer_gain,
    channel_gain,
    expert_gain,
    routes,
    route_logits,
    gate_weight,
    up_weight,
    down_weight,
):
    head_count = lambdas.shape[0]
    head_dim = head_gain.shape[0] // 2
    seq_query, seq_keys, seq_values = (
        lax.all_to_all(queries, "sp", split_axis=2, concat_axis=1, tiled=True),
        lax.all_to_all(key_rows, "sp", split_axis=2, concat_axis=1, tiled=True),
        lax.all_to_all(value_rows, "sp", split_axis=2, concat_axis=1, tiled=True),
    )
    length = seq_query.shape[1]
    query_rot = rotate(seq_query.reshape(length, head_count, 2, head_dim))
    keys_rot = rotate(seq_keys.reshape(length, head_count, 2, head_dim))
    values_heads = seq_values.reshape(length, head_count, 2 * head_dim)
    block_rows = math.gcd(length, 256)
    query_blocks = query_rot.reshape(length // block_rows, block_rows, head_count, 2, head_dim)
    scale = head_dim ** (-0.5)

    def one_block(query_block):
        scores = (
            jnp.einsum("qhcd,khcd->hcqk", query_block, keys_rot, preferred_element_type=jnp.float32)
            * scale
        )
        probs = jax.nn.softmax(scores, axis=-1)
        mixing = (probs[:, 0] - lambdas[:, None, None] * probs[:, 1]).astype(jnp.bfloat16)
        head_mix = jnp.einsum(
            "hqk,khv->qhv", mixing, values_heads, preferred_element_type=jnp.float32
        )
        return (rms_scale(head_mix, 1e-05) * head_gain).astype(jnp.bfloat16)

    head_out = lax.map(one_block, query_blocks).reshape(1, length, head_count * 2 * head_dim)
    token_rows = lax.all_to_all(head_out, "sp", split_axis=1, concat_axis=2, tiled=True)
    tokens = residual.shape[1]
    model_dim = residual.shape[2]
    projected = jnp.dot(
        token_rows.reshape(tokens, -1), out_weight, preferred_element_type=jnp.float32
    )
    stream = (
        residual.reshape(tokens, model_dim).astype(jnp.float32)
        + rms_scale(projected, 1e-06) * mixer_gain
    ).astype(jnp.bfloat16)
    normed = (rms_scale(stream.astype(jnp.float32), 1e-06) * channel_gain).astype(jnp.bfloat16)
    sp_count = lax.axis_size("sp")
    expert_count = sp_count * gate_weight.shape[0]
    capacity = max(2, 3 * tokens // expert_count)
    top_count = routes.shape[2]
    choice_ids = routes.reshape(-1)
    slots_all = choice_ids.shape[0]
    one_hot = (choice_ids[:, None] == jnp.arange(expert_count, dtype=jnp.int32)[None, :]).astype(
        jnp.int32
    )
    running = jnp.cumsum(one_hot, axis=0)
    slot_index = jnp.sum(one_hot * running, axis=1) - 1
    target = choice_ids * capacity + slot_index
    source_rows = jnp.arange(slots_all, dtype=jnp.int32) // top_count
    outgoing = (
        jnp.zeros((expert_count * capacity, model_dim), jnp.bfloat16)
        .at[target]
        .set(normed[source_rows])
    )
    outgoing = outgoing.reshape(expert_count, capacity, model_dim)
    arrived = lax.all_to_all(outgoing, "sp", split_axis=0, concat_axis=0, tiled=True).reshape(
        sp_count, 1, capacity, model_dim
    )
    expert_arrived = lax.all_gather(arrived, "dp", axis=1, tiled=True)
    shape_in = expert_arrived.shape
    flat_rows = expert_arrived.reshape(-1, shape_in[-1])
    gate_act = jnp.dot(flat_rows, gate_weight[0], preferred_element_type=jnp.float32)
    up_act = jnp.dot(flat_rows, up_weight[0], preferred_element_type=jnp.float32)
    hidden = (jax.nn.silu(gate_act) * up_act).astype(jnp.bfloat16)
    part = jnp.dot(hidden, down_weight[0], preferred_element_type=jnp.float32).astype(jnp.bfloat16)
    partial_value = part.reshape(shape_in)
    summed = lax.psum_scatter(
        partial_value.astype(jnp.float32).astype(jnp.bfloat16),
        "dp",
        scatter_dimension=1,
        tiled=True,
    )
    returned = lax.all_to_all(summed, "sp", split_axis=0, concat_axis=0, tiled=True).reshape(
        expert_count * capacity, model_dim
    )
    picked = returned[target].astype(jnp.float32).reshape(tokens, top_count, model_dim)
    shares = jax.nn.softmax(route_logits.reshape(tokens, top_count), axis=-1)
    combined = jnp.sum(picked * shares[:, :, None], axis=1)
    updated = stream.astype(jnp.float32) + rms_scale(combined, 1e-06) * expert_gain
    return updated.astype(jnp.bfloat16).reshape(1, tokens, model_dim)


def solution(mesh):
    placed = (
        P("dp", "sp", None),
        P("dp", "sp", None),
        P("dp", "sp", None),
        P("sp"),
        P(),
        P(),
        P("dp", "sp", None),
        P(),
        P(),
        P(),
        P("dp", "sp", None),
        P("dp", "sp", None),
        P("sp", None, "dp"),
        P("sp", None, "dp"),
        P("sp", "dp", None),
    )
    return jax.shard_map(
        local, mesh=mesh, in_specs=placed, out_specs=P("dp", "sp", None), check_vma=False
    )
```

profile of v0, /device:TPU:0, one launch (start us, length us, event | category | flops | bytes accessed | tf_op | source)
XLA Modules:
  0.0 459.4 jit_solution(8292478884959336948)
XLA Ops:
  6.5 2.4 copy.66
  9.5 11.5 %reduce.4 = bf16[2048,128]{1,0:T(8,128)(2,1)S(1)} reduce(bf16[2048,1,128]{2,1,0:T(2,128)(2,1)S(1)} %bitcast.147, bf16[]{:T(256)} %broadcast.286), dimensions={1}, to_apply=%bitcast.104.reduce_sub_computation | reduce | bytes 1048578
  21.0 0.9 reshape.320
  22.0 7.3 %all-to-all-start = ((bf16[8,2,16384]{2,1,0:T(2,128)(2,1)}), bf16[8,2,16384]{2,1,0:T(2,128)(2,1)S(1)}, u32[]{:S(2)}, u32[]{:S(2)}) async-start(bf16[8,2,16384]{2,1,0:T(2,128)(2,1)} %reshape.320), calls=%async_computation | async-start | bytes 1048576 | tf_op jit(solution)/shard_map/all_to_all | solution.py:49
  29.2 0.8 copy.70
  30.0 11.5 %reduce.3 = bf16[2048,128]{1,0:T(8,128)(2,1)S(1)} reduce(bf16[2048,1,128]{2,1,0:T(2,128)(2,1)S(1)} %bitcast.151, bf16[]{:T(256)} %broadcast.286), dimensions={1}, to_apply=%bitcast.106.reduce_sub_computation | reduce | bytes 1048578
  41.5 0.9 reshape.322
  42.4 1.3 all-to-all-done
  43.7 16.1 %all-to-all-start.1 = ((bf16[8,2,16384]{2,1,0:T(2,128)(2,1)}), bf16[8,2,16384]{2,1,0:T(2,128)(2,1)S(1)}, u32[]{:S(2)}, u32[]{:S(2)}) async-start(bf16[8,2,16384]{2,1,0:T(2,128)(2,1)} %reshape.322), calls=%async_computation.1 | async-start | bytes 1048576 | tf_op jit(solution)/shard_map/all_to_all | solution.py:50
  59.8 0.8 copy.72
  60.6 11.5 %reduce.5 = bf16[2048,128]{1,0:T(8,128)(2,1)S(1)} reduce(bf16[2048,1,128]{2,1,0:T(2,128)(2,1)S(1)} %bitcast.152, bf16[]{:T(256)} %broadcast.286), dimensions={1}, to_apply=%bitcast.108.reduce_sub_computation | reduce | bytes 1048578
  72.1 0.9 reshape.324
  73.9 6.0 %all-to-all-start.2 = ((bf16[8,2,16384]{2,1,0:T(2,128)(2,1)}), bf16[8,2,16384]{2,1,0:T(2,128)(2,1)}, u32[]{:S(2)}, u32[]{:S(2)}) async-start(bf16[8,2,16384]{2,1,0:T(2,128)(2,1)} %reshape.324), calls=%async_computation.2 | async-start | bytes 1048576 | tf_op jit(solution)/shard_map/all_to_all | solution.py:51
  81.4 1.1 bitcast_convert_fusion.1
  82.5 0.6 copy.67
  83.9 1.1 bitcast_convert_fusion
  85.0 0.6 copy.71
  85.8 7.6 %all-to-all-done.2 = bf16[8,2,16384]{2,1,0:T(2,128)(2,1)} async-done(((bf16[8,2,16384]{2,1,0:T(2,128)(2,1)}), bf16[8,2,16384]{2,1,0:T(2,128)(2,1)}, u32[]{:S(2)}, u32[]{:S(2)}) %all-to-all-start.2) | async-done | bytes 524320 | tf_op jit(solution)/shard_map/all_to_all | solution.py:51
  93.3 2.2 reshape.325
  96.0 1.0 reshape.266
  98.1 27.5 %while.10 = (s32[]{:T(128)}, bf16[4,256,2,128]{3,2,1,0:T(2,128)(2,1)S(1)}, bf16[4,256,2,2,64]{1,4,3,2,0:T(8,128)(2,1)S(1)}, bf16[1024,2,2,64]{0,3,2,1:T(8,128)(2...) while((s32[]{:T(128)}, ...), condition=%wide.region_4.5_spmd, body=%wide.region_0.4_spmd.sunk | while | flops 274531840 | bytes 19153508 | solution.py:73
  98.1 3.3 fusion.74
  101.4 2.6 broadcast_divide_fusion.2
  105.0 3.3 fusion.74
  108.3 2.6 broadcast_divide_fusion.2
  111.8 3.3 fusion.74
  115.1 2.6 broadcast_divide_fusion.2
  118.7 3.3 fusion.74
  122.0 2.6 broadcast_divide_fusion.2
  125.8 3.8 reduce.6
  129.6 0.9 reshape.326
  130.5 3.7 all-to-all-start.3
  134.9 13.1 %all-to-all-done.3 = bf16[8,2,16384]{2,1,0:T(2,128)(2,1)S(1)} async-done(((bf16[8,2,16384]{2,1,0:T(2,128)(2,1)}), bf16[8,2,16384]{2,1,0:T(2,128)(2,1)S(1)}, u32[]{:S(2)}, u32[]{:S(2)}) %all-to-all-start.3) | async-done | bytes 524320 | tf_op jit(solution)/shard_map/all_to_all | solution.py:74
  148.9 4.8 %multiply_reduce_fusion.4 = (f32[128]{0:T(128)S(1)}, f32[128,2048]{1,0:T(8,128)S(1)}) fusion(bf16[128,2048]{0,1:T(8,128)(2,1)S(1)} %bitcast.153, bf16[2048,2048]{1,0:T(8,128)(2,1)} %param.22), kind=kOutput, calls=%fused_computation.50 | convolution fusion | flops 1074265984 | bytes 9961984 | tf_op jit(solution)/shard_map/dot_general | solution.py:77
  154.3 5.9 %scatter_custom_fusion = bf16[384,2048]{1,0:T(8,128)(2,1)S(1)} fusion(s32[256]{0:T(256)S(1)} %bitcast.158, bf16[128,2048]{1,0:T(8,128)(2,1)S(1)} %fusion.38, s32[1024]{0:T(1024)S(1)} %pad_clamp_fusion.1, bf16[]{:T(256)} %constant.64.clone.1), kind=kCustom, calls=%fused_computation.47 | custom fusion | bytes 1572866 | tf_op jit(solution)/shard_map/scatter | solution.py:101
  160.3 39.9 %all_to_all.58 = bf16[8,48,2048]{2,1,0:T(8,128)(2,1)} all-to-all(bf16[8,48,2048]{2,1,0:T(8,128)(2,1)S(1)} %bitcast.144), channel_id=1, replica_groups=mesh['sp'=8,'dp'=4] {'sp'}, dimensions={0} | all-to-all | bytes 3145728 | tf_op jit(solution)/shard_map/all_to_all | solution.py:104
  200.6 45.1 %all-gather.3.cloned.1.call-done = bf16[8,192,2048]{2,1,0:T(8,128)(2,1)} async-done(((bf16[8,48,2048]{2,1,0:T(8,128)(2,1)}), bf16[8,192,2048]{2,1,0:T(8,128)(2,1)}) %all-gather.3.cloned.1.call-update) | async-done | bytes 6291472 | tf_op jit(solution)/shard_map/all_gather | solution.py:107
  245.7 11.6 %fusion.33 = f32[1536,1024]{1,0:T(8,128)} fusion(bf16[1536,2048]{1,0:T(8,128)(2,1)} %bitcast.162, bf16[1,2048,1024]{2,1,0:T(8,128)(2,1)} %param.29), kind=kOutput, calls=%fused_computation.34 | convolution fusion | flops 6442450944 | bytes 16777216 | tf_op jit(solution)/shard_map/dot_general | solution.py:110
  257.3 20.5 %convolution_convert_fusion = bf16[1536,2048]{1,0:T(8,128)(2,1)} fusion(bf16[1,1024,2048]{2,1,0:T(8,128)(2,1)} %param.31, f32[1536,1024]{1,0:T(8,128)} %fusion.33, bf16[1536,2048]{1,0:T(8,128)(2,1)} %bitcast.163, bf16[1,2048,1024]{2,1,0:T(8,128)(2,1)} %param.30), kind=kOutput, calls=%fused_computation.30 | convolution fusion | flops 12897484800 | bytes 27262976 | tf_op jit(solution)/shard_map/dot_general | solution.py:113
  277.9 0.6 copy-done.13
  279.1 118.5 %all-reduce.3.cloned.1.call-done = bf16[8,4,48,2048]{3,2,1,0:T(8,128)(2,1)} async-done(((bf16[8,4,48,2048]{3,2,1,0:T(8,128)(2,1)}), bf16[8,4,48,2048]{3,2,1,0:T(8,128)(2,1)}) %all-reduce.3.cloned.1.call-update) | async-done | bytes 6291472
  397.6 3.4 constant_dynamic-slice_fusion
  401.0 5.7 %all-to-all-start.5 = ((bf16[8,1,48,2048]{3,2,1,0:T(8,128)(2,1)}), bf16[8,1,48,2048]{3,2,1,0:T(8,128)(2,1)S(1)}, u32[]{:S(2)}, u32[]{:S(2)}) async-start(bf16[8,1,48,2048]{3,2,1,0:T(8,128)(2,1)} %constant_dynamic-slice_fusion), calls=%async_computation.5 | async-start | bytes 3145728 | tf_op jit(solution)/shard_map/all_to_all | solution.py:121
  406.9 36.4 %all-to-all-done.5 = bf16[8,1,48,2048]{3,2,1,0:T(8,128)(2,1)S(1)} async-done(((bf16[8,1,48,2048]{3,2,1,0:T(8,128)(2,1)}), bf16[8,1,48,2048]{3,2,1,0:T(8,128)(2,1)S(1)}, u32[]{:S(2)}, u32[]{:S(2)}) %all-to-all-start.5) | async-done | bytes 1572896 | tf_op jit(solution)/shard_map/all_to_all | solution.py:121
  443.3 2.3 gather_fusion
  445.6 2.4 reshape.280
  448.0 3.2 multiply_reduce_fusion.2
  451.3 1.0 fusion.44
  (99 shorter events, 12.6 us)
Async XLA Ops:
  6.5 22.7 %copy-start = (bf16[1,128,2048]{2,1,0:T(8,128)(2,1)S(1)}, bf16[1,128,2048]{2,1,0:T(8,128)(2,1)}, u32[]{:S(2)}) copy-start(bf16[1,128,2048]{2,1,0:T(8,128)(2,1)} %param.18) | copy-start | bytes 1572868
  9.5 50.3 %copy-start.1 = (bf16[1,128,2048]{2,1,0:T(8,128)(2,1)S(1)}, bf16[1,128,2048]{2,1,0:T(8,128)(2,1)}, u32[]{:S(2)}) copy-start(bf16[1,128,2048]{2,1,0:T(8,128)(2,1)} %param.19) | copy-start | bytes 1572868
  22.0 21.8 %all-to-all-start = ((bf16[8,2,16384]{2,1,0:T(2,128)(2,1)}), bf16[8,2,16384]{2,1,0:T(2,128)(2,1)S(1)}, u32[]{:S(2)}, u32[]{:S(2)}) async-start(bf16[8,2,16384]{2,1,0:T(2,128)(2,1)} %reshape.320), calls=%async_computation | async-start | bytes 1048576 | tf_op jit(solution)/shard_map/all_to_all | solution.py:49
  30.0 43.0 %copy-start.11 = (s32[1,128,2]{1,2,0:T(2,128)S(1)}, s32[1,128,2]{1,2,0:T(2,128)}, u32[]{:S(2)}) copy-start(s32[1,128,2]{1,2,0:T(2,128)} %param.27) | copy-start | bytes 3076
  43.7 30.1 %all-to-all-start.1 = ((bf16[8,2,16384]{2,1,0:T(2,128)(2,1)}), bf16[8,2,16384]{2,1,0:T(2,128)(2,1)S(1)}, u32[]{:S(2)}, u32[]{:S(2)}) async-start(bf16[8,2,16384]{2,1,0:T(2,128)(2,1)} %reshape.322), calls=%async_computation.1 | async-start | bytes 1048576 | tf_op jit(solution)/shard_map/all_to_all | solution.py:50
  73.9 19.5 %all-to-all-start.2 = ((bf16[8,2,16384]{2,1,0:T(2,128)(2,1)}), bf16[8,2,16384]{2,1,0:T(2,128)(2,1)}, u32[]{:S(2)}, u32[]{:S(2)}) async-start(bf16[8,2,16384]{2,1,0:T(2,128)(2,1)} %reshape.324), calls=%async_computation.2 | async-start | bytes 1048576 | tf_op jit(solution)/shard_map/all_to_all | solution.py:51
  80.3 3.6 copy-start.10
  95.6 1.9 copy-start.2
  95.7 1.9 copy-start.5
  95.7 1.9 copy-start.12
  97.0 1.0 copy-start.3
  125.5 9.2 %slice-start = ((s32[8,3]{0,1:T(4,128)}), s32[8,2]{0,1:T(2,128)S(1)}, s32[]{:S(2)}) async-start(s32[8,3]{0,1:T(4,128)} %copy-done.10), calls=%async_computation.8 | async-start | bytes 2048 | tf_op jit(solution)/shard_map/slice.1
  130.5 17.5 %all-to-all-start.3 = ((bf16[8,2,16384]{2,1,0:T(2,128)(2,1)}), bf16[8,2,16384]{2,1,0:T(2,128)(2,1)S(1)}, u32[]{:S(2)}, u32[]{:S(2)}) async-start(bf16[8,2,16384]{2,1,0:T(2,128)(2,1)} %reshape.326), calls=%async_computation.3 | async-start | bytes 1048576 | tf_op jit(solution)/shard_map/all_to_all | solution.py:74
  134.2 111.5 %all-gather.3.cloned.1.call-start = ((), (), s32[]{:S(2)}) async-start(), calls=%async_computation.6 | async-start | bytes 7864320 | tf_op jit(solution)/shard_map/all_gather | solution.py:107
  148.9 4.8 %copy-start.4 = (bf16[1,128,2048]{2,1,0:T(8,128)(2,1)S(1)}, bf16[1,128,2048]{2,1,0:T(8,128)(2,1)}, u32[]{:S(2)}) copy-start(bf16[1,128,2048]{2,1,0:T(8,128)(2,1)} %param.23) | copy-start | bytes 1572868
  148.9 4.8 %copy-start.7 = (f32[2048]{0:T(1024)S(1)}, f32[2048]{0:T(1024)}, u32[]{:S(2)}) copy-start(f32[2048]{0:T(1024)} %param.24) | copy-start | bytes 24580
  148.9 5.2 %copy-start.8 = (f32[2048]{0:T(1024)S(1)}, f32[2048]{0:T(1024)}, u32[]{:S(2)}) copy-start(f32[2048]{0:T(1024)} %param.25) | copy-start | bytes 24580
  200.2 197.4 %all-reduce.3.cloned.1.call-start = ((), (), s32[]{:S(2)}) async-start(), calls=%async_computation.7 | async-start | bytes 12582912
  277.9 0.7 copy-start.13
  277.9 128.8 %copy-start.6 = (f32[1,128,2]{1,2,0:T(2,128)S(1)}, f32[1,128,2]{1,2,0:T(2,128)}, u32[]{:S(2)}) copy-start(f32[1,128,2]{1,2,0:T(2,128)} %param.28) | copy-start | bytes 3076
  401.0 42.3 %all-to-all-start.5 = ((bf16[8,1,48,2048]{3,2,1,0:T(8,128)(2,1)}), bf16[8,1,48,2048]{3,2,1,0:T(8,128)(2,1)S(1)}, u32[]{:S(2)}, u32[]{:S(2)}) async-start(bf16[8,1,48,2048]{3,2,1,0:T(8,128)(2,1)} %constant_dynamic-slice_fusion), calls=%async_computation.5 | async-start | bytes 3145728 | tf_op jit(solution)/shard_map/all_to_all | solution.py:121
  445.6 5.7 %copy-start.9 = (f32[2048]{0:T(1024)S(1)}, f32[2048]{0:T(1024)}, u32[]{:S(2)}) copy-start(f32[2048]{0:T(1024)} %param.26) | copy-start | bytes 24580
Sparse Core Ops, SparseCore 0:
  200.3 45.3 all-gather.2
  278.0 119.5 all-reduce.2
where the time goes:
time: 468 us; the launch traced here: 459 us
  waiting for transfers between devices  222 us (47%)
  other arithmetic  58.1 us (12%)
  matrix products  52.5 us (11%)
  blocking collectives  39.9 us (9%)
  starting transfers between devices  39.5 us (8%)
  local copies, waits for them, and re-layouts  33.3 us (7%)
  between operations  14.1 us (3%)
    unnamed x3, waiting for transfers between devices  119 us
    all_gather x1, waiting for transfers between devices, local(): expert_arrived = lax.all_gather(arrived, 'dp', axis=1, tiled=True)  45.1 us
    all_to_all x1, blocking collectives, local(): lax.all_to_all(outgoing, 'sp', split_axis=0, concat_axis=0, tiled=True)  39.9 us
    unnamed x4, other arithmetic  38.3 us
    all_to_all x1, waiting for transfers between devices, local(): lax.all_to_all(summed, 'sp', split_axis=0, concat_axis=0, tiled=True)  36.4 us
    dot_general x1, matrix products, local(): jnp.dot(hidden, down_weight[0], preferred_element_type=jnp.float32)  20.5 us
    unnamed x45, local copies, waits for them, and re-layouts  17.4 us
    all_to_all x1, starting transfers between devices, local(): lax.all_to_all(key_rows, 'sp', split_axis=2, concat_axis=1, tiled=True)  16.1 us
  transfers between devices with their start and end apart: 7, of which 6 were waited for; matrix products, arithmetic and copies ran while one was open for 7% of the time, Pallas kernels for 0%

commit v1 on v0

--- a/solution.py
+++ b/solution.py
@@ -3,6 +3,16 @@
 import jax.numpy as jnp
 from jax import lax
 from jax.sharding import PartitionSpec as P
+
+
+def around_the_ring(x, mesh_axis, dim):
+    size = lax.axis_size(mesh_axis)
+    current, blocks = (x, [x])
+    for _ in range(size - 1):
+        current = lax.ppermute(current, mesh_axis, [(i, (i + 1) % size) for i in range(size)])
+        blocks.insert(0, current)
+    line = jnp.concatenate(blocks, axis=dim)
+    return jnp.roll(line, (lax.axis_index(mesh_axis) + 1) * x.shape[dim], axis=dim)
 
 
 def rotate(field):
@@ -104,7 +114,7 @@
     arrived = lax.all_to_all(outgoing, "sp", split_axis=0, concat_axis=0, tiled=True).reshape(
         sp_count, 1, capacity, model_dim
     )
-    expert_arrived = lax.all_gather(arrived, "dp", axis=1, tiled=True)
+    expert_arrived = around_the_ring(arrived, "dp", 1)
     shape_in = expert_arrived.shape
     flat_rows = expert_arrived.reshape(-1, shape_in[-1])
     gate_act = jnp.dot(flat_rows, gate_weight[0], preferred_element_type=jnp.float32)

time: 468 us -> 499 us (1.066)
  local copies, waits for them, and re-layouts: 33.3 us -> 59.8 us
  waiting for transfers between devices: 222 us -> 236 us
  starting transfers between devices: 39.5 us -> 28.2 us
    ppermute x0 -> x3, waiting for transfers between devices: none -> 59.9 us  [around_the_ring(): lax.ppermute(current, mesh_axis, [(i, (i + 1) % size) for i in range(size)])]
    all_gather x1 -> x0, waiting for transfers between devices: 45.1 us -> none  [local(): expert_arrived = lax.all_gather(arrived, 'dp', axis=1, tiled=True)]
    unnamed x45 -> x60, local copies, waits for them, and re-layouts: 17.4 us -> 35.7 us
    all_to_all x1, starting transfers between devices: 16.1 us -> 4.93 us  [local(): lax.all_to_all(key_rows, 'sp', split_axis=2, concat_axis=1, tiled=True)]
    unnamed x3 -> x2, waiting for transfers between devices: 119 us -> 118 us
  transfers between devices with their start and end apart: 7 -> 9, of which waited for: 6 -> 8; matrix products, arithmetic and copies ran while one was open for 7% -> 7% of each run, Pallas kernels for 0% -> 0%
where the time goes in v1:
time: 499 us; the launch traced here: 490 us
  waiting for transfers between devices  236 us (47%)
  local copies, waits for them, and re-layouts  59.8 us (12%)
  other arithmetic  58.2 us (12%)
  matrix products  53.5 us (11%)
  blocking collectives  39.8 us (8%)
  starting transfers between devices  28.2 us (6%)
  between operations  14.1 us (3%)
    unnamed x2, waiting for transfers between devices  118 us
    ppermute x3, waiting for transfers between devices, around_the_ring(): lax.ppermute(current, mesh_axis, [(i, (i + 1) % size) for i in range(size)])  59.9 us
    all_to_all x1, blocking collectives, local(): lax.all_to_all(outgoing, 'sp', split_axis=0, concat_axis=0, tiled=True)  39.8 us
    unnamed x4, other arithmetic  38.4 us
    all_to_all x1, waiting for transfers between devices, local(): lax.all_to_all(summed, 'sp', split_axis=0, concat_axis=0, tiled=True)  36.4 us
    unnamed x60, local copies, waits for them, and re-layouts  35.7 us
    dot_general x1, matrix products, local(): jnp.dot(hidden, down_weight[0], preferred_element_type=jnp.float32)  20.6 us
    sub x4, matrix products, one_block(): probs = jax.nn.softmax(scores, axis=-1)  13.2 us
  transfers between devices with their start and end apart: 9, of which 8 were waited for; matrix products, arithmetic and copies ran while one was open for 7% of the time, Pallas kernels for 0%

profile of v1, /device:TPU:0, one launch (start us, length us, event | category | flops | bytes accessed | tf_op | source)
XLA Modules:
  0.0 489.9 jit_solution(8319201706557502002)
XLA Ops:
  6.5 2.4 copy.66
  9.5 11.6 %reduce.4 = bf16[2048,128]{1,0:T(8,128)(2,1)S(1)} reduce(bf16[2048,1,128]{2,1,0:T(2,128)(2,1)S(1)} %bitcast.153, bf16[]{:T(256)} %broadcast.287), dimensions={1}, to_apply=%bitcast.107.reduce_sub_computation | reduce | bytes 1048578
  22.0 7.3 %all-to-all-start = ((bf16[8,2,16384]{2,1,0:T(2,128)(2,1)}), bf16[8,2,16384]{2,1,0:T(2,128)(2,1)S(1)}, u32[]{:S(2)}, u32[]{:S(2)}) async-start(bf16[8,2,16384]{2,1,0:T(2,128)(2,1)} %reshape.318), calls=%async_computation | async-start | bytes 1048576 | tf_op jit(solution)/shard_map/all_to_all | solution.py:59
  30.1 11.5 %reduce.3 = bf16[2048,128]{1,0:T(8,128)(2,1)S(1)} reduce(bf16[2048,1,128]{2,1,0:T(2,128)(2,1)S(1)} %bitcast.157, bf16[]{:T(256)} %broadcast.287), dimensions={1}, to_apply=%bitcast.109.reduce_sub_computation | reduce | bytes 1048578
  43.8 4.9 %all-to-all-start.1 = ((bf16[8,2,16384]{2,1,0:T(2,128)(2,1)}), bf16[8,2,16384]{2,1,0:T(2,128)(2,1)S(1)}, u32[]{:S(2)}, u32[]{:S(2)}) async-start(bf16[8,2,16384]{2,1,0:T(2,128)(2,1)} %reshape.320), calls=%async_computation.1 | async-start | bytes 1048576 | tf_op jit(solution)/shard_map/all_to_all | solution.py:60
  49.5 11.5 %reduce.5 = bf16[2048,128]{1,0:T(8,128)(2,1)S(1)} reduce(bf16[2048,1,128]{2,1,0:T(2,128)(2,1)S(1)} %bitcast.158, bf16[]{:T(256)} %broadcast.287), dimensions={1}, to_apply=%bitcast.111.reduce_sub_computation | reduce | bytes 1048578
  62.8 6.0 %all-to-all-start.2 = ((bf16[8,2,16384]{2,1,0:T(2,128)(2,1)}), bf16[8,2,16384]{2,1,0:T(2,128)(2,1)}, u32[]{:S(2)}, u32[]{:S(2)}) async-start(bf16[8,2,16384]{2,1,0:T(2,128)(2,1)} %reshape.322), calls=%async_computation.2 | async-start | bytes 1048576 | tf_op jit(solution)/shard_map/all_to_all | solution.py:61
  74.7 7.6 %all-to-all-done.2 = bf16[8,2,16384]{2,1,0:T(2,128)(2,1)} async-done(((bf16[8,2,16384]{2,1,0:T(2,128)(2,1)}), bf16[8,2,16384]{2,1,0:T(2,128)(2,1)}, u32[]{:S(2)}, u32[]{:S(2)}) %all-to-all-start.2) | async-done | bytes 524320 | tf_op jit(solution)/shard_map/all_to_all | solution.py:61
  82.3 2.2 reshape.323
  86.5 31.6 %while.10 = (s32[]{:T(128)}, bf16[4,256,2,128]{3,2,1,0:T(2,128)(2,1)S(1)}, bf16[4,256,2,2,64]{1,4,3,2,0:T(8,128)(2,1)S(1)}, bf16[1024,2,2,64]{0,3,2,1:T(8,128)(2...) while((s32[]{:T(128)}, ...), condition=%wide.region_4.5_spmd, body=%wide.region_0.4_spmd.sunk | while | flops 274531840 | bytes 19153508 | solution.py:83
  86.5 3.3 fusion.74
  89.8 2.6 broadcast_divide_fusion.2
  92.4 1.6 multiply_reduce_fusion.6
  94.4 3.3 fusion.74
  97.7 2.6 broadcast_divide_fusion.2
  100.3 1.6 multiply_reduce_fusion.6
  102.3 3.3 fusion.74
  105.6 2.6 broadcast_divide_fusion.2
  108.2 1.6 multiply_reduce_fusion.6
  110.2 3.3 fusion.74
  113.5 2.6 broadcast_divide_fusion.2
  116.2 1.6 multiply_reduce_fusion.6
  118.9 3.6 reshape.307
  122.5 3.8 reduce.6
  127.2 3.7 all-to-all-start.3
  131.6 13.1 %all-to-all-done.3 = bf16[8,2,16384]{2,1,0:T(2,128)(2,1)S(1)} async-done(((bf16[8,2,16384]{2,1,0:T(2,128)(2,1)}), bf16[8,2,16384]{2,1,0:T(2,128)(2,1)S(1)}, u32[]{:S(2)}, u32[]{:S(2)}) %all-to-all-start.3) | async-done | bytes 524320 | tf_op jit(solution)/shard_map/all_to_all | solution.py:84
  145.6 4.8 multiply_reduce_fusion.4
  151.6 5.9 %scatter_custom_fusion = bf16[384,2048]{1,0:T(8,128)(2,1)S(1)} fusion(s32[256]{0:T(256)S(1)} %bitcast.164, bf16[128,2048]{1,0:T(8,128)(2,1)S(1)} %fusion.38, s32[1024]{0:T(1024)S(1)} %pad_clamp_fusion.1, bf16[]{:T(256)} %constant.86.clone.1), kind=kCustom, calls=%fused_computation.47 | custom fusion | bytes 1572866 | tf_op jit(solution)/shard_map/scatter | solution.py:111
  157.5 39.8 %all_to_all.58 = bf16[8,48,2048]{2,1,0:T(8,128)(2,1)S(1)} all-to-all(bf16[8,48,2048]{2,1,0:T(8,128)(2,1)S(1)} %bitcast.150), channel_id=1, replica_groups=mesh['sp'=8,'dp'=4] {'sp'}, dimensions={0} | all-to-all | bytes 3145728 | tf_op jit(solution)/shard_map/all_to_all | solution.py:114
  197.3 19.8 %collective-permute-done = bf16[8,1,48,2048]{3,2,1,0:T(8,128)(2,1)S(1)} collective-permute-done((bf16[8,1,48,2048]{3,2,1,0:T(8,128)(2,1)S(1)}, bf16[8,1,48,2048]{3,2,1,0:T(8,128)(2,1)S(1)}, u32[]{:S(2)}, u32[]{:S(2)}) %collective-permute-start) | collective-permute-done | bytes 1572896 | tf_op jit(solution)/shard_map/ppermute | solution.py:12
  217.1 19.9 %collective-permute-done.1 = bf16[8,1,48,2048]{3,2,1,0:T(8,128)(2,1)} collective-permute-done((bf16[8,1,48,2048]{3,2,1,0:T(8,128)(2,1)S(1)}, bf16[8,1,48,2048]{3,2,1,0:T(8,128)(2,1)}, u32[]{:S(2)}, u32[]{:S(2)}) %collective-permute-start.1) | collective-permute-done | bytes 1572896 | tf_op jit(solution)/shard_map/ppermute | solution.py:12
  237.5 20.1 %collective-permute-done.2 = bf16[8,1,48,2048]{3,2,1,0:T(8,128)(2,1)} collective-permute-done((bf16[8,1,48,2048]{3,2,1,0:T(8,128)(2,1)}, bf16[8,1,48,2048]{3,2,1,0:T(8,128)(2,1)}, u32[]{:S(2)}, u32[]{:S(2)}) %collective-permute-start.2) | collective-permute-done | bytes 1572896 | tf_op jit(solution)/shard_map/ppermute | solution.py:12
  257.6 2.8 constant_dynamic-update-slice_fusion.8
  260.4 2.7 constant_dynamic-update-slice_fusion.7
  265.7 2.7 constant_dynamic-update-slice_fusion.4
  268.4 2.7 constant_dynamic-update-slice_fusion.3
  271.1 1.3 constant_dynamic-update-slice_fusion.2
  273.8 3.5 constant_dynamic-slice_fusion.1
  277.3 2.6 copy-done
  279.9 8.5 %fusion.33 = f32[1536,1024]{1,0:T(8,128)} fusion(bf16[1536,2048]{1,0:T(8,128)(2,1)S(1)} %bitcast.148, bf16[1,2048,1024]{2,1,0:T(8,128)(2,1)S(1)} %copy-done.15), kind=kOutput, calls=%fused_computation.34 | convolution fusion | flops 6442450944 | bytes 16777216 | tf_op jit(solution)/shard_map/dot_general | solution.py:120
  288.4 20.6 %convolution_convert_fusion = bf16[1536,2048]{1,0:T(8,128)(2,1)} fusion(bf16[1,1024,2048]{2,1,0:T(8,128)(2,1)} %param.31, f32[1536,1024]{1,0:T(8,128)} %fusion.33, bf16[1536,2048]{1,0:T(8,128)(2,1)} %bitcast.149, bf16[1,2048,1024]{2,1,0:T(8,128)(2,1)} %param.30), kind=kOutput, calls=%fused_computation.30 | convolution fusion | flops 12897484800 | bytes 27262976 | tf_op jit(solution)/shard_map/dot_general | solution.py:123
  310.3 117.8 %all-reduce.3.cloned.1.call-done = bf16[8,4,48,2048]{3,2,1,0:T(8,128)(2,1)} async-done(((bf16[8,4,48,2048]{3,2,1,0:T(8,128)(2,1)}), bf16[8,4,48,2048]{3,2,1,0:T(8,128)(2,1)}) %all-reduce.3.cloned.1.call-update) | async-done | bytes 6291472
  428.1 3.3 constant_dynamic-slice_fusion
  431.4 5.7 %all-to-all-start.5 = ((bf16[8,1,48,2048]{3,2,1,0:T(8,128)(2,1)}), bf16[8,1,48,2048]{3,2,1,0:T(8,128)(2,1)S(1)}, u32[]{:S(2)}, u32[]{:S(2)}) async-start(bf16[8,1,48,2048]{3,2,1,0:T(8,128)(2,1)} %constant_dynamic-slice_fusion), calls=%async_computation.5 | async-start | bytes 3145728 | tf_op jit(solution)/shard_map/all_to_all | solution.py:131
  437.3 36.4 %all-to-all-done.5 = bf16[8,1,48,2048]{3,2,1,0:T(8,128)(2,1)S(1)} async-done(((bf16[8,1,48,2048]{3,2,1,0:T(8,128)(2,1)}), bf16[8,1,48,2048]{3,2,1,0:T(8,128)(2,1)S(1)}, u32[]{:S(2)}, u32[]{:S(2)}) %all-to-all-start.5) | async-done | bytes 1572896 | tf_op jit(solution)/shard_map/all_to_all | solution.py:131
  473.7 2.3 gather_fusion
  476.1 2.4 reshape.280
  478.5 3.2 multiply_reduce_fusion.2
  (119 shorter events, 27.2 us)
Async XLA Ops:
  6.5 22.8 %copy-start.3 = (bf16[1,128,2048]{2,1,0:T(8,128)(2,1)S(1)}, bf16[1,128,2048]{2,1,0:T(8,128)(2,1)}, u32[]{:S(2)}) copy-start(bf16[1,128,2048]{2,1,0:T(8,128)(2,1)} %param.18) | copy-start | bytes 1572868
  9.5 39.2 %copy-start.4 = (bf16[1,128,2048]{2,1,0:T(8,128)(2,1)S(1)}, bf16[1,128,2048]{2,1,0:T(8,128)(2,1)}, u32[]{:S(2)}) copy-start(bf16[1,128,2048]{2,1,0:T(8,128)(2,1)} %param.19) | copy-start | bytes 1572868
  22.0 21.8 %all-to-all-start = ((bf16[8,2,16384]{2,1,0:T(2,128)(2,1)}), bf16[8,2,16384]{2,1,0:T(2,128)(2,1)S(1)}, u32[]{:S(2)}, u32[]{:S(2)}) async-start(bf16[8,2,16384]{2,1,0:T(2,128)(2,1)} %reshape.318), calls=%async_computation | async-start | bytes 1048576 | tf_op jit(solution)/shard_map/all_to_all | solution.py:59
  30.1 31.9 %copy-start.14 = (s32[1,128,2]{1,2,0:T(2,128)S(1)}, s32[1,128,2]{1,2,0:T(2,128)}, u32[]{:S(2)}) copy-start(s32[1,128,2]{1,2,0:T(2,128)} %param.27) | copy-start | bytes 3076
  43.8 19.0 %all-to-all-start.1 = ((bf16[8,2,16384]{2,1,0:T(2,128)(2,1)}), bf16[8,2,16384]{2,1,0:T(2,128)(2,1)S(1)}, u32[]{:S(2)}, u32[]{:S(2)}) async-start(bf16[8,2,16384]{2,1,0:T(2,128)(2,1)} %reshape.320), calls=%async_computation.1 | async-start | bytes 1048576 | tf_op jit(solution)/shard_map/all_to_all | solution.py:60
  62.8 19.5 %all-to-all-start.2 = ((bf16[8,2,16384]{2,1,0:T(2,128)(2,1)}), bf16[8,2,16384]{2,1,0:T(2,128)(2,1)}, u32[]{:S(2)}, u32[]{:S(2)}) async-start(bf16[8,2,16384]{2,1,0:T(2,128)(2,1)} %reshape.322), calls=%async_computation.2 | async-start | bytes 1048576 | tf_op jit(solution)/shard_map/all_to_all | solution.py:61
  69.2 3.6 copy-start.13
  84.6 1.9 copy-start.5
  84.6 1.9 copy-start.8
  84.6 1.9 copy-start.16
  118.1 0.8 copy-start.6
  118.9 12.5 %slice-start = ((s32[8,3]{0,1:T(4,128)}), s32[8,2]{0,1:T(2,128)S(1)}, s32[]{:S(2)}) async-start(s32[8,3]{0,1:T(4,128)} %copy-done.13), calls=%async_computation.7 | async-start | bytes 2048 | tf_op jit(solution)/shard_map/slice.1
  127.2 17.5 %all-to-all-start.3 = ((bf16[8,2,16384]{2,1,0:T(2,128)(2,1)}), bf16[8,2,16384]{2,1,0:T(2,128)(2,1)S(1)}, u32[]{:S(2)}, u32[]{:S(2)}) async-start(bf16[8,2,16384]{2,1,0:T(2,128)(2,1)} %reshape.324), calls=%async_computation.3 | async-start | bytes 1048576 | tf_op jit(solution)/shard_map/all_to_all | solution.py:84
  130.9 297.2 %all-reduce.3.cloned.1.call-start = ((), (), s32[]{:S(2)}) async-start(), calls=%async_computation.6 | async-start | bytes 12582912
  145.6 4.8 copy-start.7
  145.6 4.8 copy-start.10
  145.6 5.2 %copy-start.11 = (f32[2048]{0:T(1024)S(1)}, f32[2048]{0:T(1024)}, u32[]{:S(2)}) copy-start(f32[2048]{0:T(1024)} %param.25) | copy-start | bytes 24580
  150.8 0.8 copy-start.1
  197.3 19.8 %collective-permute-start = (bf16[8,1,48,2048]{3,2,1,0:T(8,128)(2,1)S(1)}, bf16[8,1,48,2048]{3,2,1,0:T(8,128)(2,1)S(1)}, u32[]{:S(2)}, u32[]{:S(2)}) collective-permute-start(bf16[8,1,48,2048]{3,2,1,0:T(8,128)(2,1)S(1)} %bitcast.146), channel_id=1, source_target_pairs={{0,1},{1,2},{2,3},{3,0},{4,5},{5,6},{6,7},{7,4},{8,9},{9,10},{10,1... | collective-permute-start | bytes 4718600 | tf_op jit(solution)/shard_map/ppermute | solution.py:12
  217.1 19.9 %collective-permute-start.1 = (bf16[8,1,48,2048]{3,2,1,0:T(8,128)(2,1)S(1)}, bf16[8,1,48,2048]{3,2,1,0:T(8,128)(2,1)}, u32[]{:S(2)}, u32[]{:S(2)}) collective-permute-start(bf16[8,1,48,2048]{3,2,1,0:T(8,128)(2,1)S(1)} %collective-permute-done), channel_id=1, source_target_pairs={{0,1},{1,2},{2,3},{3,0},{4,5},{5,6},{6,7},{7,4},{8,9},{9,10},{10,1... | collective-permute-start | bytes 4718600 | tf_op jit(solution)/shard_map/ppermute | solution.py:12
  237.1 20.5 %collective-permute-start.2 = (bf16[8,1,48,2048]{3,2,1,0:T(8,128)(2,1)}, bf16[8,1,48,2048]{3,2,1,0:T(8,128)(2,1)}, u32[]{:S(2)}, u32[]{:S(2)}) collective-permute-start(bf16[8,1,48,2048]{3,2,1,0:T(8,128)(2,1)} %collective-permute-done.1), channel_id=1, source_target_pairs={{0,1},{1,2},{2,3},{3,0},{4,5},{5,6},{6,7},{7,4},{8,9},{9,10},{10,1... | collective-permute-start | bytes 4718600 | tf_op jit(solution)/shard_map/ppermute | solution.py:12
  273.8 6.2 %copy-start.15 = (bf16[1,2048,1024]{2,1,0:T(8,128)(2,1)S(1)}, bf16[1,2048,1024]{2,1,0:T(8,128)(2,1)}, u32[]{:S(2)}) copy-start(bf16[1,2048,1024]{2,1,0:T(8,128)(2,1)} %param.29) | copy-start | bytes 12582916
  277.3 2.6 copy-start
  309.0 0.7 copy-start.17
  309.0 128.1 %copy-start.9 = (f32[1,128,2]{1,2,0:T(2,128)S(1)}, f32[1,128,2]{1,2,0:T(2,128)}, u32[]{:S(2)}) copy-start(f32[1,128,2]{1,2,0:T(2,128)} %param.28) | copy-start | bytes 3076
  431.4 42.3 %all-to-all-start.5 = ((bf16[8,1,48,2048]{3,2,1,0:T(8,128)(2,1)}), bf16[8,1,48,2048]{3,2,1,0:T(8,128)(2,1)S(1)}, u32[]{:S(2)}, u32[]{:S(2)}) async-start(bf16[8,1,48,2048]{3,2,1,0:T(8,128)(2,1)} %constant_dynamic-slice_fusion), calls=%async_computation.5 | async-start | bytes 3145728 | tf_op jit(solution)/shard_map/all_to_all | solution.py:131
  476.1 5.8 %copy-start.2 = (bf16[128,2048]{1,0:T(8,128)(2,1)S(1)}, bf16[128,2048]{1,0:T(8,128)(2,1)}, u32[]{:S(2)}) copy-start(bf16[128,2048]{1,0:T(8,128)(2,1)} %copy-done.1) | copy-start | bytes 1572868
  476.1 5.8 %copy-start.12 = (f32[2048]{0:T(1024)S(1)}, f32[2048]{0:T(1024)}, u32[]{:S(2)}) copy-start(f32[2048]{0:T(1024)} %param.26) | copy-start | bytes 24580
Sparse Core Ops, SparseCore 0:
  309.2 118.8 all-reduce.2
